TPU v7x, 32 devices: a whole 2x2x4 slice. The times are simulated.
32 devices in a mesh: sp: 8 (over z, y), tp: 4 (over x, core).
Axes of the slice: x: 2, y: 2, z: 4, core: 2. Of those that a mesh axis runs over, the one named last changes fastest.
Arguments:
- tokens: bfloat16 [4096, 2048], P('sp', 'tp'), may hold values from -64 to 64
- conv_input: bfloat16 [2048, 1024], P(None, 'tp'), may hold values from -0.125 to 0.125
- conv_inner: bfloat16 [2048, 1024], P(None, 'tp'), may hold values from -0.125 to 0.125
- conv_outer: bfloat16 [2048, 1024], P(None, 'tp'), may hold values from -0.125 to 0.125
- conv_gate: bfloat16 [2048, 1024], P(None, 'tp'), may hold values from -0.125 to 0.125
- conv_taps: bfloat16 [3, 1024], P(None, 'tp'), may hold values from -3.5 to 3.5
- query_proj: bfloat16 [2048, 1536], P(None, 'tp'), may hold values from -8 to 8
- latent_proj: bfloat16 [2048, 256], replicated, may hold values from -1 to 1
- rope_proj: bfloat16 [2048, 32], replicated, may hold values from -0.125 to 0.125
- latent_gain: float32 [256], replicated, may hold values from 0.1 to 1.9
- key_up: bfloat16 [256, 1024], P(None, 'tp'), may hold values from -2 to 2
- value_up: bfloat16 [256, 1024], P(None, 'tp'), may hold values from -0.375 to 0.375
- attn_gate: bfloat16 [2048, 1024], P(None, 'tp'), may hold values from -0.125 to 0.125
- conv_down: bfloat16 [1024, 2048], P('tp'), may hold values from -0.1875 to 0.1875
- attn_down: bfloat16 [1024, 2048], P('tp'), may hold values from -0.75 to 0.75
Outputs:
- layer_out: bfloat16 [4096, 2048], P(('sp', 'tp'))
All inputs are finite; a program needn't handle non-finite values.
Results may differ from a plain program's by a relative error of at most 0.014.
Values may be sent and summed in bfloat16 or wider, within the bound.
A program may use at most 128 MiB of HBM per device.

v0:
```python
import functools
import math

import jax
import jax.numpy as jnp
from jax import lax
from jax.experimental import pallas as pl
from jax.experimental.pallas import tpu as pltpu
from jax.sharding import PartitionSpec as P

NOPE = 64
ROPE = 32
VDIM = 64
VROWS = VDIM + 16
HW = NOPE + ROPE
GRID_W = 64
LANES = 128
EDGE = 16
rms_eps = 1e-06
rope_theta = 10000.0
MESH = pl.DeviceIdType.MESH
BF = jnp.bfloat16
F32 = jnp.float32


def silu(v):
    return v / (1.0 + jnp.exp(-v))


def dot(a, b):
    return jnp.dot(a, b, preferred_element_type=F32)


def dot_t(a, b):
    return lax.dot_general(a, b, (((1,), (1,)), ((), ())), preferred_element_type=F32)


def flip(a, s):
    out, bit = a, 1
    while bit <= s:
        if s & bit:
            out = out + bit * (1 - 2 * ((a // bit) % 2))
        bit *= 2
    return out


def body(
    dims,
    tokens, wci, wcn, wco, wcg, wq, wg, wl, wr, cd, ad, ku, vu, taps, gain,
    out,
    x_all, w_conv, w_q, w_g, w_l, w_r, w_k, w_v, v_t, w_down, kv, kn, kr, vt, qbuf, cosb, sina, sinb, tab,
    cprod, cgo, gat, halo, mix, mbuf, acc, sbuf, send_b, pbuf, xbuf, rbuf, ybuf,
    wsem, tsend, trecv, rsend, rrecv, zsend, zrecv, ysend, yrecv, msend, mrecv, hsend, hrecv,
    dsend, drecv, xsend, xrecv,
):
    n_sp, n_tp, Y, Z, R, fl, D, H, C, KV, NC, NP, KB = dims
    X = n_tp // 2
    RG = R // X
    TB = R // n_tp
    RC = R // NC
    RP = RC // 4
    A = H * VDIM
    KC = n_sp * RC
    DP = D // NP
    sp = lax.axis_index("sp")
    tp = lax.axis_index("tp")
    chip = tp // 2
    core = tp % 2
    mate = chip * 2 + (1 - core)
    zi = sp // Y
    yi = sp % Y

    loads = [
        pltpu.make_async_copy(wl, w_l, wsem.at[0]),
        pltpu.make_async_copy(wr, w_r, wsem.at[1]),
        pltpu.make_async_copy(wq, w_q, wsem.at[2]),
        pltpu.make_async_copy(wcn, w_conv.at[0], wsem.at[3]),
        pltpu.make_async_copy(wci, w_conv.at[1], wsem.at[4]),
        pltpu.make_async_copy(wco, w_conv.at[2], wsem.at[5]),
        pltpu.make_async_copy(wcg, w_conv.at[3], wsem.at[6]),
        pltpu.make_async_copy(wg, w_g, wsem.at[7]),
        pltpu.make_async_copy(ku, w_k, wsem.at[8]),
        pltpu.make_async_copy(vu, w_v, wsem.at[9]),
        pltpu.make_async_copy(cd, w_down.at[0:C, :], wsem.at[10]),
        pltpu.make_async_copy(ad, w_down.at[C:, :], wsem.at[11]),
    ]

    def cols(j):
        return pl.ds(pl.multiple_of(j * fl, fl), fl)

    own = pltpu.make_async_copy(tokens, x_all.at[:, cols(tp)], wsem.at[12])

    barrier = pltpu.get_barrier_semaphore()
    pl.semaphore_signal(barrier, inc=1, device_id={"tp": mate}, device_id_type=MESH)
    for d in range(1, X):
        peer = ((chip + d) % X) * 2 + core
        pl.semaphore_signal(barrier, inc=1, device_id={"tp": peer}, device_id_type=MESH)
    for d in range(1, n_sp):
        pl.semaphore_signal(barrier, inc=1, device_id={"sp": (sp + d) % n_sp}, device_id_type=MESH)
    own.start()
    for w in loads:
        w.start()

    lane = lax.broadcasted_iota(jnp.int32, (R, LANES), 1)
    pos = sp * R + lax.broadcasted_iota(jnp.int32, (R, LANES), 0)
    grid = jnp.where(lane < ROPE // 2, pos // GRID_W, pos % GRID_W).astype(F32)
    ang = grid * jnp.exp((lane % 8).astype(F32) * (-math.log(rope_theta) / 8.0))
    active = lane < ROPE
    first = (lane % 16) < 8
    sin = jnp.sin(ang)
    cosb[...] = jnp.where(active, jnp.cos(ang), 0.0)
    sina[...] = jnp.where(active & first, -sin, 0.0)
    sinb[...] = jnp.where(active & (~first), sin, 0.0)
    post = sp * R + lax.broadcasted_iota(jnp.int32, (8, R), 1)
    freq = jnp.exp(lax.broadcasted_iota(jnp.int32, (8, R), 0).astype(F32) * (-math.log(rope_theta) / 8.0))
    rang = (post // GRID_W).astype(F32) * freq
    cang = (post % GRID_W).astype(F32) * freq
    tab[0] = jnp.cos(rang)
    tab[1] = jnp.sin(rang)
    tab[2] = jnp.cos(cang)
    tab[3] = jnp.sin(cang)

    qbuf[...] = jnp.zeros(qbuf.shape, BF)
    ones = jnp.where(lax.broadcasted_iota(jnp.int32, (VROWS - VDIM, n_sp * R), 0) == 0, 1.0, 0.0).astype(BF)
    for h in range(H):
        vt[h, VDIM:VROWS, :] = ones
    mbuf[...] = jnp.full(mbuf.shape, -jnp.inf, F32)
    acc[...] = jnp.zeros(acc.shape, F32)

    pl.semaphore_wait(barrier, 1 + (X - 1) + (n_sp - 1))

    def send_tok(d, c):
        peer = mate if d == 0 else ((chip + d) % X) * 2 + core
        rows = pl.ds(c * RC, RC)
        return pltpu.make_async_remote_copy(
            src_ref=tokens.at[rows], dst_ref=x_all.at[rows, cols(tp)],
            send_sem=tsend.at[d, c], recv_sem=trecv.at[d, c],
            device_id={"tp": peer}, device_id_type=MESH)

    def relay_tok(d, c):
        origin = ((chip - d + X) % X) * 2 + core
        rows = pl.ds(c * RC, RC)
        part = x_all.at[rows, cols(origin)]
        return pltpu.make_async_remote_copy(
            src_ref=part, dst_ref=part,
            send_sem=rsend.at[d, c], recv_sem=rrecv.at[d, c],
            device_id={"tp": mate}, device_id_type=MESH)

    for c in range(NC):
        for d in range(1, X):
            send_tok(d, c).start()
    for c in range(NC):
        send_tok(0, c).start()

    def send_z(c, s):
        part = kv.at[c, core, yi, zi]
        return pltpu.make_async_remote_copy(
            src_ref=part, dst_ref=part, send_sem=zsend.at[c, s], recv_sem=zrecv.at[c, s],
            device_id={"sp": flip(zi, s) * Y + yi}, device_id_type=MESH)

    def send_y(c, t, s):
        part = kv.at[c, core, yi, flip(zi, s)]
        return pltpu.make_async_remote_copy(
            src_ref=part, dst_ref=part, send_sem=ysend.at[c, t, s], recv_sem=yrecv.at[c, t, s],
            device_id={"sp": zi * Y + flip(yi, t)}, device_id_type=MESH)

    def send_m(c, t, s):
        part = kv.at[c, core, flip(yi, t), flip(zi, s)]
        return pltpu.make_async_remote_copy(
            src_ref=part, dst_ref=part, send_sem=msend.at[c, t, s], recv_sem=mrecv.at[c, t, s],
            device_id={"tp": mate}, device_id_type=MESH)

    def kv_start(c):
        for s in range(1, Z):
            send_z(c, s).start()
        for t in range(1, Y):
            send_y(c, t, 0).start()
        send_m(c, 0, 0).start()

    def kv_line(c, s):
        send_z(c, s).wait_recv()
        for t in range(1, Y):
            send_y(c, t, s).start()
        send_m(c, 0, s).start()

    def kv_cross(c, s):
        for t in range(1, Y):
            send_y(c, t, s).wait_recv()
            send_m(c, t, s).start()

    def kv_done(c):
        for t in range(Y):
            for s in range(Z):
                send_m(c, t, s).wait_recv()

    def turned(v, rows):
        return (v * cosb[rows, :] + pltpu.roll(v, LANES - 8, 1) * sina[rows, :]
                + pltpu.roll(v, 8, 1) * sinb[rows, :])

    def row_scale(c):
        xf = x_all[c * RC:(c + 1) * RC, :].astype(F32)
        return lax.rsqrt(jnp.sum(xf * xf, axis=1, keepdims=True) * (1.0 / D) + rms_eps)

    def latents(c, sc):
        rows = pl.ds(c * RC, RC)
        xr = x_all[rows, :]
        lat = dot(xr, w_l[...]) * sc
        lat = lat * lax.rsqrt(jnp.mean(lat * lat, axis=1, keepdims=True) + rms_eps) * gain[...]
        rp = jnp.concatenate([dot(xr, w_r[...]) * sc, jnp.zeros((RC, LANES - ROPE), F32)], axis=1)
        rp = turned(rp, rows)
        packed = rp[0:RP]
        for g in range(1, 4):
            packed = packed + pltpu.roll(rp[g * RP:(g + 1) * RP], 32 * g, 1)
        kv[c, core, yi, zi, 0:RC, :] = jnp.where(core == 0, lat[:, 0:LANES], lat[:, LANES:]).astype(BF)
        kv[c, core, yi, zi, RC:, :] = jnp.where(core == 0, packed[0:RP // 2], packed[RP // 2:]).astype(BF)

    scale = HW ** -0.5 * math.log2(math.e)

    def queries(c, sc):
        rows = pl.ds(c * RC, RC)
        q = dot(x_all[rows, :], w_q[...]) * (sc * scale)
        width = q.shape[1]
        if width % LANES:
            q = jnp.concatenate([q, jnp.zeros((RC, LANES - width % LANES), F32)], axis=1)
        qt = q.T
        blk, off = (c * RC) // RG, (c * RC) % RG
        cr, sr, cc, sn = [tab[i, :, c * RC:(c + 1) * RC] for i in range(4)]
        for h in range(H):
            low = (h % 2) * NOPE
            at = h * HW
            a, b, e, f = [qt[at + NOPE + 8 * i:at + NOPE + 8 * (i + 1)] for i in range(4)]
            qbuf[blk, h, low:low + NOPE, off:off + RC] = qt[at:at + NOPE].astype(BF)
            qbuf[blk, h, LANES:LANES + ROPE, off:off + RC] = jnp.concatenate(
                [a * cr - b * sr, b * cr + a * sr, e * cc - f * sn, f * cc + e * sn], axis=0).astype(BF)

    def conv_in(c, sc):
        rows = pl.ds(c * RC, RC)
        xr = x_all[rows, :]
        inner = (dot(xr, w_conv[0]) * sc).astype(BF).astype(F32)
        value = (dot(xr, w_conv[1]) * sc).astype(BF).astype(F32)
        cprod[rows, :] = (inner * value).astype(BF)
        outer = (dot(xr, w_conv[2]) * sc).astype(BF).astype(F32)
        gate = (dot(xr, w_conv[3]) * sc).astype(BF).astype(F32)
        cgo[rows, :] = silu(gate) * outer

    def gate_in(c, sc):
        rows = pl.ds(c * RC, RC)
        gat[rows, :] = silu((dot(x_all[rows, :], w_g[...]) * sc).astype(BF).astype(F32))

    def send_halo(k):
        src = cprod.at[pl.ds(R - EDGE, EDGE)] if k == 0 else cprod.at[pl.ds(0, EDGE)]
        to = (sp + 1) % n_sp if k == 0 else (sp + n_sp - 1) % n_sp
        return pltpu.make_async_remote_copy(
            src_ref=src, dst_ref=halo.at[k], send_sem=hsend.at[k], recv_sem=hrecv.at[k],
            device_id={"sp": to}, device_id_type=MESH)

    def build(c):
        k0 = c * KC
        for o in range(n_sp):
            y, z = o // Z, o % Z
            r0 = k0 + o * RC
            lat = jnp.concatenate([kv[c, 0, y, z, 0:RC, :], kv[c, 1, y, z, 0:RC, :]], axis=1)
            pk = jnp.concatenate([kv[c, 0, y, z, RC:, :], kv[c, 1, y, z, RC:, :]], axis=0).astype(F32)
            kr[r0:r0 + RC, :] = jnp.concatenate(
                [pk if g == 0 else pltpu.roll(pk, LANES - 32 * g, 1) for g in range(4)], axis=0).astype(BF)
            kn[r0:r0 + RC, :] = dot(lat, w_k[...]).astype(BF)
            v = dot_t(v_t[...], lat).astype(BF)
            for h in range(H):
                vt[h, 0:VDIM, r0:r0 + RC] = v[h * VDIM:(h + 1) * VDIM]

    def attend(kq, c):
        units = [(h, j) for j in range(KC // KB) for h in range(H)]
        n = len(units)

        def score(u):
            h, j = units[u]
            rows = pl.ds(c * KC + j * KB, KB)
            p = (h // 2) * LANES
            k = jnp.concatenate([kn[rows, p:p + LANES], kr[rows, :]], axis=1)
            sbuf[u % 3] = dot(k, qbuf[kq, h])

        def top(u):
            h, _ = units[u]
            old = mbuf[kq, h]
            new = jnp.maximum(old, jnp.max(sbuf[u % 3], axis=0, keepdims=True))
            mbuf[kq, h] = new
            return new, jnp.exp2(old - new)

        def weigh(u, p, shrink):
            h, j = units[u]
            acc[kq, h] = acc[kq, h] * shrink + dot(vt[h, :, c * KC + j * KB:c * KC + (j + 1) * KB], p)

        score(0)
        if n > 1:
            score(1)
        tops = {0: top(0)}
        last = None
        for u in range(n):
            if u + 2 < n:
                score(u + 2)
            if last is not None:
                weigh(*last)
            if u + 1 < n:
                tops[u + 1] = top(u + 1)
            new, shrink = tops.pop(u)
            last = (u, jnp.exp2(sbuf[u % 3] - new).astype(BF), shrink)
        weigh(*last)

    def finish(kq):
        rows = pl.ds(pl.multiple_of(kq * RG, RG), RG)
        heads = []
        for h in range(H):
            a = acc[kq, h]
            heads.append(a[0:VDIM] / a[VDIM:VDIM + 1])
        attended = jnp.concatenate(heads, axis=0).T
        mix[rows, C:] = (gat[rows, :] * attended).astype(BF)

    def send_mate(d, i):
        return pltpu.make_async_remote_copy(
            src_ref=send_b.at[d, i], dst_ref=pbuf.at[d, i], send_sem=dsend.at[d, i], recv_sem=drecv.at[d, i],
            device_id={"tp": mate}, device_id_type=MESH)

    def send_x(d, i):
        return pltpu.make_async_remote_copy(
            src_ref=xbuf.at[d, i], dst_ref=rbuf.at[d, i], send_sem=xsend.at[d, i], recv_sem=xrecv.at[d, i],
            device_id={"tp": ((chip + d) % X) * 2 + core}, device_id_type=MESH)

    def block(kq, which, i):
        rows = pl.ds(pl.multiple_of(kq * RG + which * TB, TB), TB)
        return dot(mix[rows, :], w_down[:, i * DP:(i + 1) * DP]).astype(BF)

    def pair_sum(d, i):
        send_mate(d, i).wait_recv()
        return ybuf[i].astype(F32) + pbuf[d, i].astype(F32)

    def project_out(d):
        kq = (chip + d) % X

        def push(i):
            xbuf[d, i] = pair_sum(d, i).astype(BF)
            send_x(d, i).start()

        for i in range(NP):
            send_b[d, i] = block(kq, 1 - core, i)
            send_mate(d, i).start()
            ybuf[i] = block(kq, core, i)
            if d and i:
                push(i - 1)
        if d:
            push(NP - 1)

    def conv_out():
        send_halo(0).wait_recv()
        send_halo(1).wait_recv()
        cp = cprod[...].astype(F32)
        rid = lax.broadcasted_iota(jnp.int32, (R, C), 0)
        before = halo[0].astype(F32)[EDGE - 1:EDGE, :] * jnp.where(sp == 0, 0.0, 1.0)
        after = halo[1].astype(F32)[0:1, :] * jnp.where(sp == n_sp - 1, 0.0, 1.0)
        up = jnp.where(rid == 0, before, pltpu.roll(cp, 1, 0))
        down = jnp.where(rid == R - 1, after, pltpu.roll(cp, R - 1, 0))
        tw = taps[...].astype(F32)
        mix[:, 0:C] = (cgo[...] * (up * tw[0:1] + cp * tw[1:2] + down * tw[2:3])).astype(BF)

    near = [s for s in range(1, Z) if s < 2]
    far = [s for s in range(1, Z) if s >= 2]

    own.wait()
    loads[0].wait()
    loads[1].wait()
    for c in range(NC):
        for d in range(1, X):
            send_tok(d, c).wait_recv()
            relay_tok(d, c).start()
        send_tok(0, c).wait_recv()
        for d in range(1, X):
            relay_tok(d, c).wait_recv()
        sc = row_scale(c)
        latents(c, sc)
        kv_start(c)
        if c == 0:
            for w in loads[2:]:
                w.wait()
            v_t[...] = w_v[...].astype(F32).T.astype(BF)
        queries(c, sc)
        gate_in(c, sc)
        conv_in(c, sc)
        if c >= 2:
            for s in far:
                kv_line(c - 2, s)
            kv_cross(c - 2, 0)
        if c >= 1:
            for s in near:
                kv_line(c - 1, s)
        if c >= 3:
            for s in range(1, Z):
                kv_cross(c - 3, s)
    send_halo(0).start()
    send_halo(1).start()

    first_q = (chip + 1) % X
    last_q = chip
    for s in far:
        kv_line(NC - 2, s)
    kv_cross(NC - 2, 0)
    for s in range(1, Z):
        kv_cross(NC - 3, s)
    kv_done(0)
    build(0)
    attend(first_q, 0)
    for s in near:
        kv_line(NC - 1, s)
    kv_done(1)
    build(1)
    for s in range(1, Z):
        kv_cross(NC - 2, s)
    for s in far:
        kv_line(NC - 1, s)
    kv_cross(NC - 1, 0)
    attend(first_q, 1)
    for s in range(1, Z):
        kv_cross(NC - 1, s)
    kv_done(2)
    build(2)
    attend(first_q, 2)
    conv_out()
    kv_done(3)
    build(3)
    attend(first_q, 3)
    finish(first_q)
    for d in range(1, X):
        project_out(d)
        kq = (chip + d + 1) % X
        for c in range(NC):
            attend(kq, c)
        finish(kq)
    project_out(0)

    for i in range(NP):
        total = pair_sum(0, i)
        for d in range(1, X):
            send_x(d, i).wait_recv()
            total = total + rbuf[d, i].astype(F32)
        out[:, i * DP:(i + 1) * DP] = total.astype(BF)

    for c in range(NC):
        send_tok(0, c).wait_send()
        for d in range(1, X):
            send_tok(d, c).wait_send()
            relay_tok(d, c).wait_send()
        for s in range(Z):
            if s:
                send_z(c, s).wait_send()
            for t in range(Y):
                if t:
                    send_y(c, t, s).wait_send()
                send_m(c, t, s).wait_send()
    send_halo(0).wait_send()
    send_halo(1).wait_send()
    for i in range(NP):
        for d in range(X):
            send_mate(d, i).wait_send()
            if d:
                send_x(d, i).wait_send()


def on_device(n_sp, n_tp, tokens, wci, wcn, wco, wcg, taps, wq, wl, wr, gain, ku, vu, wg, cd, ad):
    R, fl = tokens.shape
    D, C = wci.shape
    KV = wl.shape[1]
    H = ku.shape[1] // NOPE
    A = H * VDIM
    X = n_tp // 2
    Y = X if n_sp % X == 0 else 1
    Z = n_sp // Y
    RG, TB = R // X, R // n_tp
    NC, NP = 4, 4
    RC = R // NC
    DP = D // NP
    S = n_sp * R
    KB = min(512, n_sp * RC)
    dma = pltpu.SemaphoreType.DMA
    anys = pl.BlockSpec(memory_space=pl.ANY)
    vm = pl.BlockSpec(memory_space=pltpu.VMEM)
    V = pltpu.VMEM
    return pl.pallas_call(
        functools.partial(body, (n_sp, n_tp, Y, Z, R, fl, D, H, C, KV, NC, NP, KB)),
        out_shape=jax.ShapeDtypeStruct((TB, cd.shape[1]), BF),
        in_specs=[anys] * 13 + [vm] * 2,
        out_specs=vm,
        scratch_shapes=[
            V((R, D), BF), V((4, D, C), BF), V(wq.shape, BF), V((D, A), BF),
            V((D, KV), BF), V(wr.shape, BF), V(ku.shape, BF), V(vu.shape, BF),
            V((A, KV), BF), V((C + A, cd.shape[1]), BF),
            V((NC, 2, Y, Z, RC + RC // 8, LANES), BF),
            V((S, H * NOPE), BF), V((S, LANES), BF), V((H, VROWS, S), BF), V((X, H, 2 * LANES, RG), BF),
            V((R, LANES), F32), V((R, LANES), F32), V((R, LANES), F32), V((4, 8, R), F32),
            V((R, C), BF), V((R, C), F32), V((R, A), F32), V((2, EDGE, C), BF), V((R, C + A), BF),
            V((X, H, 1, RG), F32), V((X, H, VROWS, RG), F32), V((3, KB, RG), F32),
            V((X, NP, TB, DP), BF), V((X, NP, TB, DP), BF),
            V((X, NP, TB, DP), BF), V((X, NP, TB, DP), BF), V((NP, TB, DP), BF),
            dma((13,)), dma((X, NC)), dma((X, NC)), dma((X, NC)), dma((X, NC)),
            dma((NC, Z)), dma((NC, Z)), dma((NC, Y, Z)), dma((NC, Y, Z)), dma((NC, Y, Z)), dma((NC, Y, Z)),
            dma((2,)), dma((2,)),
            dma((X, NP)), dma((X, NP)), dma((X, NP)), dma((X, NP)),
        ],
        compiler_params=pltpu.CompilerParams(
            collective_id=0, has_side_effects=True, vmem_limit_bytes=60 * 1024 * 1024),
    )(tokens, wci, wcn, wco, wcg, wq, wg, wl, wr, cd, ad, ku, vu, taps, gain.reshape(1, KV))


def solution(mesh):
    tp = P(None, "tp")
    placed = (P("sp", "tp"), tp, tp, tp, tp, tp, tp, P(), P(), P(), tp, tp, tp,
              P("tp", None), P("tp", None))
    return jax.shard_map(
        functools.partial(on_device, mesh.shape["sp"], mesh.shape["tp"]),
        mesh=mesh, in_specs=placed, out_specs=P(("sp", "tp"), None), check_vma=False)
```

profile of v0, /device:TPU:0, one launch (start us, length us, event | category | flops | bytes accessed | tf_op | source)
XLA Modules:
  0.0 60.5 jit_solution(13633544265498483781)
XLA Ops:
  0.0 1.9 %copy.16.wr = bf16[2048,32]{1,0:T(8,128)(2,1)} copy(bf16[2048,32]{0,1:T(8,128)(2,1)} %param.23) | data formatting | bytes 262144 | tf_op args[8]
  1.9 56.7 %shard_map.145 = bf16[128,2048]{1,0:T(8,128)(2,1)} custom-call(bf16[512,512]{1,0:T(8,128)(2,1)} %tokens.1, bf16[2048,256]{1,0:T(8,128)(2,1)} %wci.1, bf16[2048,256]{1,0:T(8,128)(2,1)} %wcn.1, bf16[2048,256]{1,0:T(8,128)(2,1)} %wco.1, bf16[2048,256]{1,0:T(8,128)(2,1)} %wcg.1, bf16[2048,384]{1,0:T(8,128)(2,1)} %wq.1, bf16[2048,256]{1,0:T(8,128)(2,1)} %wg.1, ...), custom_call_target="tpu_custom_call" | custom-call | tf_op jit(solution)/shard_map/pallas_call | solution.py:485
  58.6 1.9 %copy.18 = bf16[128,2048]{1,0:T(8,128)(2,1)} copy(bf16[128,2048]{1,0:T(8,128)(2,1)} %shard_map.145) | data formatting | bytes 1048576
where the time goes:
time: 60.7 us; the launch traced here: 60.5 us
  Pallas kernels  56.7 us (93%)
  local copies, waits for them, and re-layouts  3.79 us (6%)
    pallas_call x1, Pallas kernels, on_device(): pl.pallas_call(functools.partial(body, (n_sp, n_tp, Y, Z, R, fl, D, H, C,...  56.7 us
    unnamed x2, local copies, waits for them, and re-layouts  3.79 us

commit v1 on v0

--- a/solution.py
+++ b/solution.py
@@ -49,9 +49,9 @@
     tokens, wci, wcn, wco, wcg, wq, wg, wl, wr, cd, ad, ku, vu, taps, gain,
     out,
     x_all, w_conv, w_q, w_g, w_l, w_r, w_k, w_v, v_t, w_down, kv, kn, kr, vt, qbuf, cosb, sina, sinb, tab,
-    cprod, cgo, gat, halo, mix, mbuf, acc, sbuf, send_b, pbuf, xbuf, rbuf, ybuf,
+    cprod, cgo, gat, halo, mix, mbuf, acc, sbuf, send_b, pbuf, xbuf, rbuf, ybuf, obuf, zp, rpp, ssq,
     wsem, tsend, trecv, rsend, rrecv, zsend, zrecv, ysend, yrecv, msend, mrecv, hsend, hrecv,
-    dsend, drecv, xsend, xrecv,
+    dsend, drecv, xsend, xrecv, osem,
 ):
     n_sp, n_tp, Y, Z, R, fl, D, H, C, KV, NC, NP, KB = dims
     X = n_tp // 2
@@ -98,7 +98,7 @@
     for d in range(1, n_sp):
         pl.semaphore_signal(barrier, inc=1, device_id={"sp": (sp + d) % n_sp}, device_id_type=MESH)
     own.start()
-    for w in loads:
+    for w in loads[0:2]:
         w.start()
 
     lane = lax.broadcasted_iota(jnp.int32, (R, LANES), 1)
@@ -133,8 +133,8 @@
         peer = mate if d == 0 else ((chip + d) % X) * 2 + core
         rows = pl.ds(c * RC, RC)
         return pltpu.make_async_remote_copy(
-            src_ref=tokens.at[rows], dst_ref=x_all.at[rows, cols(tp)],
-            send_sem=tsend.at[d, c], recv_sem=trecv.at[d, c],
+            src_ref=x_all.at[rows, cols(tp)], dst_ref=x_all.at[rows, cols(tp)],
+            send_sem=tsend.at[d], recv_sem=trecv.at[d, c],
             device_id={"tp": peer}, device_id_type=MESH)
 
     def relay_tok(d, c):
@@ -143,31 +143,34 @@
         part = x_all.at[rows, cols(origin)]
         return pltpu.make_async_remote_copy(
             src_ref=part, dst_ref=part,
-            send_sem=rsend.at[d, c], recv_sem=rrecv.at[d, c],
+            send_sem=rsend.at[d], recv_sem=rrecv.at[d, c],
             device_id={"tp": mate}, device_id_type=MESH)
 
+    own.wait()
     for c in range(NC):
         for d in range(1, X):
             send_tok(d, c).start()
     for c in range(NC):
         send_tok(0, c).start()
+    for w in loads[2:]:
+        w.start()
 
     def send_z(c, s):
         part = kv.at[c, core, yi, zi]
         return pltpu.make_async_remote_copy(
-            src_ref=part, dst_ref=part, send_sem=zsend.at[c, s], recv_sem=zrecv.at[c, s],
+            src_ref=part, dst_ref=part, send_sem=zsend.at[0], recv_sem=zrecv.at[c, s],
             device_id={"sp": flip(zi, s) * Y + yi}, device_id_type=MESH)
 
     def send_y(c, t, s):
         part = kv.at[c, core, yi, flip(zi, s)]
         return pltpu.make_async_remote_copy(
-            src_ref=part, dst_ref=part, send_sem=ysend.at[c, t, s], recv_sem=yrecv.at[c, t, s],
+            src_ref=part, dst_ref=part, send_sem=ysend.at[0], recv_sem=yrecv.at[c, t, s],
             device_id={"sp": zi * Y + flip(yi, t)}, device_id_type=MESH)
 
     def send_m(c, t, s):
         part = kv.at[c, core, flip(yi, t), flip(zi, s)]
         return pltpu.make_async_remote_copy(
-            src_ref=part, dst_ref=part, send_sem=msend.at[c, t, s], recv_sem=mrecv.at[c, t, s],
+            src_ref=part, dst_ref=part, send_sem=msend.at[0], recv_sem=mrecv.at[c],
             device_id={"tp": mate}, device_id_type=MESH)
 
     def kv_start(c):
@@ -188,31 +191,46 @@
             send_y(c, t, s).wait_recv()
             send_m(c, t, s).start()
 
+    def lines(c, peers):
+        for s in peers:
+            kv_line(c, s)
+
+    def crosses(c, peers):
+        for s in peers:
+            kv_cross(c, s)
+
     def kv_done(c):
-        for t in range(Y):
-            for s in range(Z):
-                send_m(c, t, s).wait_recv()
+        part = kv.at[c, 1 - core]
+        pltpu.make_async_remote_copy(
+            src_ref=part, dst_ref=part, send_sem=msend.at[0], recv_sem=mrecv.at[c],
+            device_id={"tp": mate}, device_id_type=MESH).wait_recv()
 
     def turned(v, rows):
         return (v * cosb[rows, :] + pltpu.roll(v, LANES - 8, 1) * sina[rows, :]
                 + pltpu.roll(v, 8, 1) * sinb[rows, :])
 
-    def row_scale(c):
-        xf = x_all[c * RC:(c + 1) * RC, :].astype(F32)
-        return lax.rsqrt(jnp.sum(xf * xf, axis=1, keepdims=True) * (1.0 / D) + rms_eps)
-
-    def latents(c, sc):
-        rows = pl.ds(c * RC, RC)
-        xr = x_all[rows, :]
-        lat = dot(xr, w_l[...]) * sc
+    def feature_part(rows, j):
+        xr = x_all[rows, cols(j)]
+        xf = xr.astype(F32)
+        return (dot(xr, w_l[cols(j), :]), dot_t(xr, w_r[:, cols(j)]), jnp.sum(xf * xf, axis=1, keepdims=True))
+
+    def add_parts(parts):
+        return tuple(functools.reduce(lambda u, v: u + v, p) for p in zip(*parts))
+
+    def latents(c, parts):
+        rows = pl.ds(c * RC, RC)
+        lat, rope, total = add_parts([(zp[rows, :], rpp[rows, :], ssq[rows, :])] + parts)
+        sc = lax.rsqrt(total * (1.0 / D) + rms_eps)
+        lat = lat * sc
         lat = lat * lax.rsqrt(jnp.mean(lat * lat, axis=1, keepdims=True) + rms_eps) * gain[...]
-        rp = jnp.concatenate([dot(xr, w_r[...]) * sc, jnp.zeros((RC, LANES - ROPE), F32)], axis=1)
+        kv[c, core, yi, zi, 0:RC, :] = jnp.where(core == 0, lat[:, 0:LANES], lat[:, LANES:]).astype(BF)
+        rp = jnp.concatenate([rope * sc, jnp.zeros((RC, LANES - ROPE), F32)], axis=1)
         rp = turned(rp, rows)
         packed = rp[0:RP]
         for g in range(1, 4):
             packed = packed + pltpu.roll(rp[g * RP:(g + 1) * RP], 32 * g, 1)
-        kv[c, core, yi, zi, 0:RC, :] = jnp.where(core == 0, lat[:, 0:LANES], lat[:, LANES:]).astype(BF)
         kv[c, core, yi, zi, RC:, :] = jnp.where(core == 0, packed[0:RP // 2], packed[RP // 2:]).astype(BF)
+        return sc
 
     scale = HW ** -0.5 * math.log2(math.e)
 
@@ -256,21 +274,29 @@
 
     def build(c):
         k0 = c * KC
-        for o in range(n_sp):
-            y, z = o // Z, o % Z
-            r0 = k0 + o * RC
-            lat = jnp.concatenate([kv[c, 0, y, z, 0:RC, :], kv[c, 1, y, z, 0:RC, :]], axis=1)
-            pk = jnp.concatenate([kv[c, 0, y, z, RC:, :], kv[c, 1, y, z, RC:, :]], axis=0).astype(F32)
-            kr[r0:r0 + RC, :] = jnp.concatenate(
-                [pk if g == 0 else pltpu.roll(pk, LANES - 32 * g, 1) for g in range(4)], axis=0).astype(BF)
-            kn[r0:r0 + RC, :] = dot(lat, w_k[...]).astype(BF)
+        n = max(1, KB // RC)
+        for g0 in range(0, n_sp, n):
+            lats = []
+            for o in range(g0, g0 + n):
+                y, z = o // Z, o % Z
+                r0 = k0 + o * RC
+                lats.append(jnp.concatenate([kv[c, 0, y, z, 0:RC, :], kv[c, 1, y, z, 0:RC, :]], axis=1))
+                pk = jnp.concatenate([kv[c, 0, y, z, RC:, :], kv[c, 1, y, z, RC:, :]], axis=0).astype(F32)
+                kr[r0:r0 + RC, :] = jnp.concatenate(
+                    [pk if g == 0 else pltpu.roll(pk, LANES - 32 * g, 1) for g in range(4)], axis=0).astype(BF)
+            lat = jnp.concatenate(lats, axis=0)
+            r0 = k0 + g0 * RC
+            kn[r0:r0 + n * RC, :] = dot(lat, w_k[...]).astype(BF)
             v = dot_t(v_t[...], lat).astype(BF)
             for h in range(H):
-                vt[h, 0:VDIM, r0:r0 + RC] = v[h * VDIM:(h + 1) * VDIM]
-
-    def attend(kq, c):
+                vt[h, 0:VDIM, r0:r0 + n * RC] = v[h * VDIM:(h + 1) * VDIM]
+
+    def attend(kq, c, part=None):
         units = [(h, j) for j in range(KC // KB) for h in range(H)]
         n = len(units)
+        if part is not None:
+            units = units[part * (n // 2):(part + 1) * (n // 2)]
+            n = len(units)
 
         def score(u):
             h, j = units[u]
@@ -317,12 +343,12 @@
 
     def send_mate(d, i):
         return pltpu.make_async_remote_copy(
-            src_ref=send_b.at[d, i], dst_ref=pbuf.at[d, i], send_sem=dsend.at[d, i], recv_sem=drecv.at[d, i],
+            src_ref=send_b.at[d, i], dst_ref=pbuf.at[d, i], send_sem=dsend.at[d], recv_sem=drecv.at[d, i],
             device_id={"tp": mate}, device_id_type=MESH)
 
     def send_x(d, i):
         return pltpu.make_async_remote_copy(
-            src_ref=xbuf.at[d, i], dst_ref=rbuf.at[d, i], send_sem=xsend.at[d, i], recv_sem=xrecv.at[d, i],
+            src_ref=xbuf.at[d, i], dst_ref=rbuf.at[d, i], send_sem=xsend.at[d], recv_sem=xrecv.at[d, i],
             device_id={"tp": ((chip + d) % X) * 2 + core}, device_id_type=MESH)
 
     def block(kq, which, i):
@@ -333,6 +359,9 @@
         send_mate(d, i).wait_recv()
         return ybuf[i].astype(F32) + pbuf[d, i].astype(F32)
 
+    def give(i):
+        return pltpu.make_async_copy(obuf.at[i], out.at[:, i * DP:(i + 1) * DP], osem.at[i])
+
     def project_out(d):
         kq = (chip + d) % X
 
@@ -343,11 +372,10 @@
         for i in range(NP):
             send_b[d, i] = block(kq, 1 - core, i)
             send_mate(d, i).start()
+        for i in range(NP):
             ybuf[i] = block(kq, core, i)
-            if d and i:
-                push(i - 1)
-        if d:
-            push(NP - 1)
+            if d:
+                push(i)
 
     def conv_out():
         send_halo(0).wait_recv()
@@ -364,65 +392,72 @@
     near = [s for s in range(1, Z) if s < 2]
     far = [s for s in range(1, Z) if s >= 2]
 
-    own.wait()
     loads[0].wait()
     loads[1].wait()
+    every = pl.ds(0, R)
+    parts = [feature_part(every, tp)]
     for c in range(NC):
+        send_tok(0, c).wait_recv()
+    parts.append(feature_part(every, mate))
+    zp[...], rpp[...], ssq[...] = add_parts(parts)
+
+    scales = []
+    for c in range(NC):
+        rows = pl.ds(c * RC, RC)
+        parts = []
         for d in range(1, X):
             send_tok(d, c).wait_recv()
             relay_tok(d, c).start()
-        send_tok(0, c).wait_recv()
-        for d in range(1, X):
-            relay_tok(d, c).wait_recv()
-        sc = row_scale(c)
-        latents(c, sc)
-        kv_start(c)
-        if c == 0:
+            parts.append(feature_part(rows, ((chip - d + X) % X) * 2 + core))
+        if c == 1:
             for w in loads[2:]:
                 w.wait()
             v_t[...] = w_v[...].astype(F32).T.astype(BF)
-        queries(c, sc)
-        gate_in(c, sc)
-        conv_in(c, sc)
+        if c:
+            conv_in(c - 1, scales[c - 1])
+        for d in range(1, X):
+            relay_tok(d, c).wait_recv()
+            parts.append(feature_part(rows, ((chip - d + X) % X) * 2 + 1 - core))
+        scales.append(latents(c, parts))
+        kv_start(c)
+        if c:
+            queries(c - 1, scales[c - 1])
+            gate_in(c - 1, scales[c - 1])
+        if c >= 1:
+            lines(c - 1, near)
         if c >= 2:
-            for s in far:
-                kv_line(c - 2, s)
-            kv_cross(c - 2, 0)
-        if c >= 1:
-            for s in near:
-                kv_line(c - 1, s)
+            crosses(c - 2, [0] + near)
+            lines(c - 2, far)
         if c >= 3:
-            for s in range(1, Z):
-                kv_cross(c - 3, s)
-    send_halo(0).start()
-    send_halo(1).start()
+            crosses(c - 3, far)
+    queries(NC - 1, scales[NC - 1])
+    gate_in(NC - 1, scales[NC - 1])
 
     first_q = (chip + 1) % X
-    last_q = chip
-    for s in far:
-        kv_line(NC - 2, s)
-    kv_cross(NC - 2, 0)
-    for s in range(1, Z):
-        kv_cross(NC - 3, s)
     kv_done(0)
     build(0)
     attend(first_q, 0)
-    for s in near:
-        kv_line(NC - 1, s)
+    lines(3, near)
+    crosses(2, [0] + near)
+    lines(2, far)
+    crosses(1, far)
+    crosses(3, [0])
+    conv_in(NC - 1, scales[NC - 1])
+    send_halo(0).start()
+    send_halo(1).start()
     kv_done(1)
     build(1)
-    for s in range(1, Z):
-        kv_cross(NC - 2, s)
-    for s in far:
-        kv_line(NC - 1, s)
-    kv_cross(NC - 1, 0)
-    attend(first_q, 1)
-    for s in range(1, Z):
-        kv_cross(NC - 1, s)
+    attend(first_q, 1, 0)
+    crosses(3, near)
+    attend(first_q, 1, 1)
+    lines(3, far)
+    crosses(2, far)
+    conv_out()
     kv_done(2)
     build(2)
-    attend(first_q, 2)
-    conv_out()
+    attend(first_q, 2, 0)
+    crosses(3, far)
+    attend(first_q, 2, 1)
     kv_done(3)
     build(3)
     attend(first_q, 3)
@@ -440,29 +475,25 @@
         for d in range(1, X):
             send_x(d, i).wait_recv()
             total = total + rbuf[d, i].astype(F32)
-        out[:, i * DP:(i + 1) * DP] = total.astype(BF)
-
-    for c in range(NC):
-        send_tok(0, c).wait_send()
-        for d in range(1, X):
-            send_tok(d, c).wait_send()
-            relay_tok(d, c).wait_send()
-        for s in range(Z):
-            if s:
-                send_z(c, s).wait_send()
-            for t in range(Y):
-                if t:
-                    send_y(c, t, s).wait_send()
-                send_m(c, t, s).wait_send()
+        obuf[i] = total.astype(BF)
+        give(i).start()
+
+    def sent(ref, sem):
+        pltpu.make_async_copy(ref, ref, sem).wait()
+
+    for d in range(X):
+        sent(x_all.at[:, cols(tp)], tsend.at[d])
+        sent(send_b.at[d], dsend.at[d])
+        if d:
+            sent(x_all.at[:, cols(tp)], rsend.at[d])
+            sent(xbuf.at[d], xsend.at[d])
+    sent(kv.at[:, core, 0, pl.ds(0, Z - 1)], zsend.at[0])
+    sent(kv.at[:, core, pl.ds(0, Y - 1)], ysend.at[0])
+    sent(kv.at[:, core], msend.at[0])
     send_halo(0).wait_send()
     send_halo(1).wait_send()
     for i in range(NP):
-        for d in range(X):
-            send_mate(d, i).wait_send()
-            if d:
-                send_x(d, i).wait_send()
-
-
+        give(i).wait()
 def on_device(n_sp, n_tp, tokens, wci, wcn, wco, wcg, taps, wq, wl, wr, gain, ku, vu, wg, cd, ad):
     R, fl = tokens.shape
     D, C = wci.shape
@@ -486,10 +517,10 @@
         functools.partial(body, (n_sp, n_tp, Y, Z, R, fl, D, H, C, KV, NC, NP, KB)),
         out_shape=jax.ShapeDtypeStruct((TB, cd.shape[1]), BF),
         in_specs=[anys] * 13 + [vm] * 2,
-        out_specs=vm,
+        out_specs=anys,
         scratch_shapes=[
             V((R, D), BF), V((4, D, C), BF), V(wq.shape, BF), V((D, A), BF),
-            V((D, KV), BF), V(wr.shape, BF), V(ku.shape, BF), V(vu.shape, BF),
+            V((D, KV), BF), V((ROPE, D), BF), V(ku.shape, BF), V(vu.shape, BF),
             V((A, KV), BF), V((C + A, cd.shape[1]), BF),
             V((NC, 2, Y, Z, RC + RC // 8, LANES), BF),
             V((S, H * NOPE), BF), V((S, LANES), BF), V((H, VROWS, S), BF), V((X, H, 2 * LANES, RG), BF),
@@ -497,15 +528,16 @@
             V((R, C), BF), V((R, C), F32), V((R, A), F32), V((2, EDGE, C), BF), V((R, C + A), BF),
             V((X, H, 1, RG), F32), V((X, H, VROWS, RG), F32), V((3, KB, RG), F32),
             V((X, NP, TB, DP), BF), V((X, NP, TB, DP), BF),
-            V((X, NP, TB, DP), BF), V((X, NP, TB, DP), BF), V((NP, TB, DP), BF),
-            dma((13,)), dma((X, NC)), dma((X, NC)), dma((X, NC)), dma((X, NC)),
-            dma((NC, Z)), dma((NC, Z)), dma((NC, Y, Z)), dma((NC, Y, Z)), dma((NC, Y, Z)), dma((NC, Y, Z)),
+            V((X, NP, TB, DP), BF), V((X, NP, TB, DP), BF), V((NP, TB, DP), BF), V((NP, TB, DP), BF),
+            V((R, KV), F32), V((R, ROPE), F32), V((R, 1), F32),
+            dma((13,)), dma((X,)), dma((X, NC)), dma((X,)), dma((X, NC)),
+            dma((1,)), dma((NC, Z)), dma((1,)), dma((NC, Y, Z)), dma((1,)), dma((NC,)),
             dma((2,)), dma((2,)),
-            dma((X, NP)), dma((X, NP)), dma((X, NP)), dma((X, NP)),
+            dma((X,)), dma((X, NP)), dma((X,)), dma((X, NP)), dma((NP,)),
         ],
         compiler_params=pltpu.CompilerParams(
             collective_id=0, has_side_effects=True, vmem_limit_bytes=60 * 1024 * 1024),
-    )(tokens, wci, wcn, wco, wcg, wq, wg, wl, wr, cd, ad, ku, vu, taps, gain.reshape(1, KV))
+    )(tokens, wci, wcn, wco, wcg, wq, wg, wl, wr.T, cd, ad, ku, vu, taps, gain.reshape(1, KV))
 
 
 def solution(mesh):

time: 60.7 us -> 55.6 us (0.916)
  Pallas kernels: 56.7 us -> 53.6 us
  local copies, waits for them, and re-layouts: 3.79 us -> 1.88 us
    pallas_call x1, Pallas kernels: 56.7 us -> 53.6 us  [on_device(): pl.pallas_call(functools.partial(body, (n_sp, n_tp, Y, Z, R, fl, D, H, C,...]
    unnamed x2 -> x1, local copies, waits for them, and re-layouts: 3.79 us -> 1.88 us
where the time goes in v1:
time: 55.6 us; the launch traced here: 55.4 us
  Pallas kernels  53.6 us (96%)
  local copies, waits for them, and re-layouts  1.88 us (3%)
    pallas_call x1, Pallas kernels, on_device(): pl.pallas_call(functools.partial(body, (n_sp, n_tp, Y, Z, R, fl, D, H, C,...  53.6 us
    unnamed x1, local copies, waits for them, and re-layouts  1.88 us

profile of v1, /device:TPU:0, one launch (start us, length us, event | category | flops | bytes accessed | tf_op | source)
XLA Modules:
  0.0 55.4 jit_solution(10500627153175898296)
XLA Ops:
  0.0 53.6 %shard_map.145 = bf16[128,2048]{1,0:T(8,128)(2,1)} custom-call(bf16[512,512]{1,0:T(8,128)(2,1)} %tokens.1, bf16[2048,256]{1,0:T(8,128)(2,1)} %wci.1, bf16[2048,256]{1,0:T(8,128)(2,1)} %wcn.1, bf16[2048,256]{1,0:T(8,128)(2,1)} %wco.1, bf16[2048,256]{1,0:T(8,128)(2,1)} %wcg.1, bf16[2048,384]{1,0:T(8,128)(2,1)} %wq.1, bf16[2048,256]{1,0:T(8,128)(2,1)} %wg.1, ...), custom_call_target="tpu_custom_call" | custom-call | tf_op jit(solution)/shard_map/pallas_call | solution.py:516
  53.6 1.9 %copy.17 = bf16[128,2048]{1,0:T(8,128)(2,1)} copy(bf16[128,2048]{1,0:T(8,128)(2,1)} %shard_map.145) | data formatting | bytes 1048576

commit v2 on v1

v2 whole, which is shorter than its diff:
```python
import functools
import math

import jax
import jax.numpy as jnp
from jax import lax
from jax.experimental import pallas as pl
from jax.experimental.pallas import tpu as pltpu
from jax.sharding import PartitionSpec as P

NOPE = 64
ROPE = 32
VDIM = 64
VROWS = VDIM + 16
HW = NOPE + ROPE
GRID_W = 64
LANES = 128
EDGE = 16
rms_eps = 1e-06
rope_theta = 10000.0
MESH = pl.DeviceIdType.MESH
BF = jnp.bfloat16
F32 = jnp.float32


def silu(v):
    return v / (1.0 + jnp.exp(-v))


def dot(a, b):
    return jnp.dot(a, b, preferred_element_type=F32)


def dot_t(a, b):
    return lax.dot_general(a, b, (((1,), (1,)), ((), ())), preferred_element_type=F32)


def flip(a, s):
    out, bit = a, 1
    while bit <= s:
        if s & bit:
            out = out + bit * (1 - 2 * ((a // bit) % 2))
        bit *= 2
    return out


def body(
    dims,
    tokens, wci, wcn, wco, wcg, wq, wg, wl, wr, cd, ad, ku, vu, taps, gain,
    out,
    x_all, w_conv, w_q, w_g, w_l, w_r, w_k, w_v, v_t, w_down, kv, kn, kr, vt, qbuf, cosb, sina, sinb, tab,
    cprod, cgo, gat, halo, mix, mbuf, acc, sbuf, send_b, pbuf, xbuf, rbuf, ybuf, obuf, zp, rpp, ssq,
    wsem, tsend, trecv, rsend, rrecv, zsend, zrecv, ysend, yrecv, msend, mrecv, hsend, hrecv,
    dsend, drecv, xsend, xrecv, osem,
):
    n_sp, n_tp, Y, Z, R, fl, D, H, C, KV, NC, NP, KB = dims
    X = n_tp // 2
    RG = R // X
    TB = R // n_tp
    RC = R // NC
    RP = RC // 4
    A = H * VDIM
    KC = n_sp * RC
    DP = D // NP
    sp = lax.axis_index("sp")
    tp = lax.axis_index("tp")
    chip = tp // 2
    core = tp % 2
    mate = chip * 2 + (1 - core)
    zi = sp // Y
    yi = sp % Y

    loads = [
        pltpu.make_async_copy(wl, w_l, wsem.at[0]),
        pltpu.make_async_copy(wr, w_r, wsem.at[1]),
        pltpu.make_async_copy(wq, w_q, wsem.at[2]),
        pltpu.make_async_copy(wcn, w_conv.at[0], wsem.at[3]),
        pltpu.make_async_copy(wci, w_conv.at[1], wsem.at[4]),
        pltpu.make_async_copy(wco, w_conv.at[2], wsem.at[5]),
        pltpu.make_async_copy(wcg, w_conv.at[3], wsem.at[6]),
        pltpu.make_async_copy(wg, w_g, wsem.at[7]),
        pltpu.make_async_copy(ku, w_k, wsem.at[8]),
        pltpu.make_async_copy(vu, w_v, wsem.at[9]),
        pltpu.make_async_copy(cd, w_down.at[0:C, :], wsem.at[10]),
        pltpu.make_async_copy(ad, w_down.at[C:, :], wsem.at[11]),
    ]

    def cols(j):
        return pl.ds(pl.multiple_of(j * fl, fl), fl)

    own = pltpu.make_async_copy(tokens, x_all.at[:, cols(tp)], wsem.at[12])

    barrier = pltpu.get_barrier_semaphore()
    pl.semaphore_signal(barrier, inc=1, device_id={"tp": mate}, device_id_type=MESH)
    for d in range(1, X):
        peer = ((chip + d) % X) * 2 + core
        pl.semaphore_signal(barrier, inc=1, device_id={"tp": peer}, device_id_type=MESH)
    for d in range(1, n_sp):
        pl.semaphore_signal(barrier, inc=1, device_id={"sp": (sp + d) % n_sp}, device_id_type=MESH)
    own.start()
    for w in loads[0:2]:
        w.start()

    pl.semaphore_wait(barrier, 1 + (X - 1) + (n_sp - 1))

    BC = NC // X

    def rows_for(to, c):
        return pl.ds(pl.multiple_of((((to + 1) * BC + c) % NC) * RC, RC), RC)

    def rows_of(c):
        return rows_for(chip, c)

    def send_tok(d, c):
        to = (chip + d) % X
        peer = mate if d == 0 else to * 2 + core
        rows = rows_for(to, c)
        return pltpu.make_async_remote_copy(
            src_ref=x_all.at[rows, cols(tp)], dst_ref=x_all.at[rows, cols(tp)],
            send_sem=tsend.at[d], recv_sem=trecv.at[d, c],
            device_id={"tp": peer}, device_id_type=MESH)

    def relay_tok(d, c):
        origin = ((chip - d + X) % X) * 2 + core
        rows = rows_of(c)
        part = x_all.at[rows, cols(origin)]
        return pltpu.make_async_remote_copy(
            src_ref=part, dst_ref=part,
            send_sem=rsend.at[d], recv_sem=rrecv.at[d, c],
            device_id={"tp": mate}, device_id_type=MESH)

    own.wait()
    for c in range(NC):
        for d in range(1, X):
            send_tok(d, c).start()
    for c in range(NC):
        send_tok(0, c).start()
    for w in loads[2:]:
        w.start()

    def send_z(c, s):
        part = kv.at[c, core, yi, zi]
        return pltpu.make_async_remote_copy(
            src_ref=part, dst_ref=part, send_sem=zsend.at[0], recv_sem=zrecv.at[c, s],
            device_id={"sp": flip(zi, s) * Y + yi}, device_id_type=MESH)

    def send_y(c, t, s):
        part = kv.at[c, core, yi, flip(zi, s)]
        return pltpu.make_async_remote_copy(
            src_ref=part, dst_ref=part, send_sem=ysend.at[0], recv_sem=yrecv.at[c, t, s],
            device_id={"sp": zi * Y + flip(yi, t)}, device_id_type=MESH)

    def send_m(c, t, s):
        part = kv.at[c, core, flip(yi, t), flip(zi, s)]
        return pltpu.make_async_remote_copy(
            src_ref=part, dst_ref=part, send_sem=msend.at[0], recv_sem=mrecv.at[c, t],
            device_id={"tp": mate}, device_id_type=MESH)

    def kv_start(c):
        for s in range(1, Z):
            send_z(c, s).start()
        for t in range(1, Y):
            send_y(c, t, 0).start()
        send_m(c, 0, 0).start()

    def kv_line(c, s):
        send_z(c, s).wait_recv()
        for t in range(1, Y):
            send_y(c, t, s).start()
        send_m(c, 0, s).start()

    def kv_cross(c, s):
        for t in range(1, Y):
            send_y(c, t, s).wait_recv()
            send_m(c, t, s).start()

    def lines(c, peers):
        for s in peers:
            kv_line(c, s)

    def crosses(c, peers):
        for s in peers:
            kv_cross(c, s)

    def kv_done(c, t):
        part = kv.at[c, 1 - core, flip(yi, t)]
        pltpu.make_async_remote_copy(
            src_ref=part, dst_ref=part, send_sem=msend.at[0], recv_sem=mrecv.at[c, t],
            device_id={"tp": mate}, device_id_type=MESH).wait_recv()

    def turned(v, rows):
        return (v * cosb[rows, :] + pltpu.roll(v, LANES - 8, 1) * sina[rows, :]
                + pltpu.roll(v, 8, 1) * sinb[rows, :])

    def feature_part(rows, j):
        xr = x_all[rows, cols(j)]
        xf = xr.astype(F32)
        return (dot(xr, w_l[cols(j), :]), dot_t(xr, w_r[:, cols(j)]), jnp.sum(xf * xf, axis=1, keepdims=True))

    def add_parts(parts):
        return tuple(functools.reduce(lambda u, v: u + v, p) for p in zip(*parts))

    def latents(c, parts):
        rows = rows_of(c)
        lat, rope, total = add_parts([(zp[rows, :], rpp[rows, :], ssq[rows, :])] + parts)
        sc = lax.rsqrt(total * (1.0 / D) + rms_eps)
        lat = lat * sc
        lat = lat * lax.rsqrt(jnp.mean(lat * lat, axis=1, keepdims=True) + rms_eps) * gain[...]
        kv[c, core, yi, zi, 0:RC, :] = jnp.where(core == 0, lat[:, 0:LANES], lat[:, LANES:]).astype(BF)
        rp = jnp.concatenate([rope * sc, jnp.zeros((RC, LANES - ROPE), F32)], axis=1)
        rp = turned(rp, rows)
        packed = rp[0:RP]
        for g in range(1, 4):
            packed = packed + pltpu.roll(rp[g * RP:(g + 1) * RP], 32 * g, 1)
        kv[c, core, yi, zi, RC:, :] = jnp.where(core == 0, packed[0:RP // 2], packed[RP // 2:]).astype(BF)
        return sc

    scale = HW ** -0.5 * math.log2(math.e)

    def queries(c, sc):
        rows = rows_of(c)
        q = dot(x_all[rows, :], w_q[...]) * (sc * scale)
        width = q.shape[1]
        if width % LANES:
            q = jnp.concatenate([q, jnp.zeros((RC, LANES - width % LANES), F32)], axis=1)
        qt = q.T
        blk, off = (chip + 1 + c // BC) % X, (c % BC) * RC
        cr, sr, cc, sn = [tab[i, :, rows] for i in range(4)]
        for h in range(H):
            low = (h % 2) * NOPE
            at = h * HW
            a, b, e, f = [qt[at + NOPE + 8 * i:at + NOPE + 8 * (i + 1)] for i in range(4)]
            qbuf[blk, h, low:low + NOPE, off:off + RC] = qt[at:at + NOPE].astype(BF)
            qbuf[blk, h, LANES:LANES + ROPE, off:off + RC] = jnp.concatenate(
                [a * cr - b * sr, b * cr + a * sr, e * cc - f * sn, f * cc + e * sn], axis=0).astype(BF)

    def conv_in(c, sc):
        rows = rows_of(c)
        xr = x_all[rows, :]
        inner = (dot(xr, w_conv[0]) * sc).astype(BF).astype(F32)
        value = (dot(xr, w_conv[1]) * sc).astype(BF).astype(F32)
        cprod[rows, :] = (inner * value).astype(BF)
        outer = (dot(xr, w_conv[2]) * sc).astype(BF).astype(F32)
        gate = (dot(xr, w_conv[3]) * sc).astype(BF).astype(F32)
        cgo[rows, :] = silu(gate) * outer

    def gate_in(c, sc):
        rows = rows_of(c)
        gat[rows, :] = silu((dot(x_all[rows, :], w_g[...]) * sc).astype(BF).astype(F32))

    def send_halo(k):
        src = cprod.at[pl.ds(R - EDGE, EDGE)] if k == 0 else cprod.at[pl.ds(0, EDGE)]
        to = (sp + 1) % n_sp if k == 0 else (sp + n_sp - 1) % n_sp
        return pltpu.make_async_remote_copy(
            src_ref=src, dst_ref=halo.at[k], send_sem=hsend.at[k], recv_sem=hrecv.at[k],
            device_id={"sp": to}, device_id_type=MESH)

    def build(c, t):
        kv_done(c, t)
        y = flip(yi, t)
        n = max(1, min(KB // RC, Z))
        for g0 in range(0, Z, n):
            k0 = pl.multiple_of((c * Y + y) * (Z * RC) + g0 * RC, n * RC)
            lats, ropes = [], []
            for z in range(g0, g0 + n):
                lats.append(jnp.concatenate([kv[c, 0, y, z, 0:RC, :], kv[c, 1, y, z, 0:RC, :]], axis=1))
                pk = jnp.concatenate([kv[c, 0, y, z, RC:, :], kv[c, 1, y, z, RC:, :]], axis=0).astype(F32)
                ropes += [pk if g == 0 else pltpu.roll(pk, LANES - 32 * g, 1) for g in range(4)]
            lat = jnp.concatenate(lats, axis=0)
            rows = pl.ds(k0, n * RC)
            kr[rows, :] = jnp.concatenate(ropes, axis=0).astype(BF)
            kn[rows, :] = dot(lat, w_k[...]).astype(BF)
            v = dot_t(v_t[...], lat).astype(BF)
            for h in range(H):
                vt[h, 0:VDIM, rows] = v[h * VDIM:(h + 1) * VDIM]

    def attend(kq, blocks):
        units = [(h, k0 + j * KB) for k0, count in blocks for j in range(count // KB) for h in range(H)]
        n = len(units)

        def score(u):
            h, k0 = units[u]
            rows = pl.ds(pl.multiple_of(k0, KB), KB)
            p = (h // 2) * LANES
            k = jnp.concatenate([kn[rows, p:p + LANES], kr[rows, :]], axis=1)
            sbuf[u % 3] = dot(k, qbuf[kq, h])

        def top(u):
            h, _ = units[u]
            old = mbuf[kq, h]
            new = jnp.maximum(old, jnp.max(sbuf[u % 3], axis=0, keepdims=True))
            mbuf[kq, h] = new
            return new, jnp.exp2(old - new)

        def weigh(u, p, shrink):
            h, k0 = units[u]
            acc[kq, h] = acc[kq, h] * shrink + dot(vt[h, :, pl.ds(pl.multiple_of(k0, KB), KB)], p)

        score(0)
        if n > 1:
            score(1)
        tops = {0: top(0)}
        last = None
        for u in range(n):
            if u + 2 < n:
                score(u + 2)
            if last is not None:
                weigh(*last)
            if u + 1 < n:
                tops[u + 1] = top(u + 1)
            new, shrink = tops.pop(u)
            last = (u, jnp.exp2(sbuf[u % 3] - new).astype(BF), shrink)
        weigh(*last)

    def line(c, t):
        return ((c * Y + flip(yi, t)) * (Z * RC), Z * RC)

    def chunks(kq, a, b):
        attend(kq, [(c * KC, KC) for c in range(a, b)])

    cross = list(range(1, Y))

    def take(c, peers):
        for t in peers:
            build(c, t)

    def heed(kq, c, peers):
        if peers:
            attend(kq, [line(c, t) for t in peers])

    def finish(kq):
        rows = pl.ds(pl.multiple_of(kq * RG, RG), RG)
        heads = []
        for h in range(H):
            a = acc[kq, h]
            heads.append(a[0:VDIM] / a[VDIM:VDIM + 1])
        attended = jnp.concatenate(heads, axis=0).T
        mix[rows, C:] = (gat[rows, :] * attended).astype(BF)

    def send_mate(d, i):
        return pltpu.make_async_remote_copy(
            src_ref=send_b.at[d, i], dst_ref=pbuf.at[d, i], send_sem=dsend.at[d], recv_sem=drecv.at[d, i],
            device_id={"tp": mate}, device_id_type=MESH)

    def send_x(d, i):
        return pltpu.make_async_remote_copy(
            src_ref=xbuf.at[d, i], dst_ref=rbuf.at[d, i], send_sem=xsend.at[d], recv_sem=xrecv.at[d, i],
            device_id={"tp": ((chip + d) % X) * 2 + core}, device_id_type=MESH)

    def block(kq, which, i):
        rows = pl.ds(pl.multiple_of(kq * RG + which * TB, TB), TB)
        return dot(mix[rows, :], w_down[:, i * DP:(i + 1) * DP]).astype(BF)

    def pair_sum(d, i):
        send_mate(d, i).wait_recv()
        return ybuf[i].astype(F32) + pbuf[d, i].astype(F32)

    def give(i):
        return pltpu.make_async_copy(obuf.at[i], out.at[:, i * DP:(i + 1) * DP], osem.at[i])

    def project_out(d):
        kq = (chip + d) % X

        def push(i):
            xbuf[d, i] = pair_sum(d, i).astype(BF)
            send_x(d, i).start()

        for i in range(NP):
            send_b[d, i] = block(kq, 1 - core, i)
            send_mate(d, i).start()
        for i in range(NP):
            ybuf[i] = block(kq, core, i)
            if d:
                push(i)

    def conv_out():
        send_halo(0).wait_recv()
        send_halo(1).wait_recv()
        cp = cprod[...].astype(F32)
        rid = lax.broadcasted_iota(jnp.int32, (R, C), 0)
        before = halo[0].astype(F32)[EDGE - 1:EDGE, :] * jnp.where(sp == 0, 0.0, 1.0)
        after = halo[1].astype(F32)[0:1, :] * jnp.where(sp == n_sp - 1, 0.0, 1.0)
        up = jnp.where(rid == 0, before, pltpu.roll(cp, 1, 0))
        down = jnp.where(rid == R - 1, after, pltpu.roll(cp, R - 1, 0))
        tw = taps[...].astype(F32)
        mix[:, 0:C] = (cgo[...] * (up * tw[0:1] + cp * tw[1:2] + down * tw[2:3])).astype(BF)

    near = [s for s in range(1, Z) if s < 2]
    far = [s for s in range(1, Z) if s >= 2]

    loads[0].wait()
    loads[1].wait()
    every = pl.ds(0, R)
    parts = [feature_part(every, tp)]
    for c in range(NC):
        send_tok(0, c).wait_recv()
    parts.append(feature_part(every, mate))
    zp[...], rpp[...], ssq[...] = add_parts(parts)

    lane = lax.broadcasted_iota(jnp.int32, (R, LANES), 1)
    pos = sp * R + lax.broadcasted_iota(jnp.int32, (R, LANES), 0)
    grid = jnp.where(lane < ROPE // 2, pos // GRID_W, pos % GRID_W).astype(F32)
    ang = grid * jnp.exp((lane % 8).astype(F32) * (-math.log(rope_theta) / 8.0))
    active = lane < ROPE
    first = (lane % 16) < 8
    sin = jnp.sin(ang)
    cosb[...] = jnp.where(active, jnp.cos(ang), 0.0)
    sina[...] = jnp.where(active & first, -sin, 0.0)
    sinb[...] = jnp.where(active & (~first), sin, 0.0)
    post = sp * R + lax.broadcasted_iota(jnp.int32, (8, R), 1)
    freq = jnp.exp(lax.broadcasted_iota(jnp.int32, (8, R), 0).astype(F32) * (-math.log(rope_theta) / 8.0))
    rang = (post // GRID_W).astype(F32) * freq
    cang = (post % GRID_W).astype(F32) * freq
    tab[0] = jnp.cos(rang)
    tab[1] = jnp.sin(rang)
    tab[2] = jnp.cos(cang)
    tab[3] = jnp.sin(cang)

    qbuf[...] = jnp.zeros(qbuf.shape, BF)
    ones = jnp.where(lax.broadcasted_iota(jnp.int32, (VROWS - VDIM, n_sp * R), 0) == 0, 1.0, 0.0).astype(BF)
    for h in range(H):
        vt[h, VDIM:VROWS, :] = ones
    mbuf[...] = jnp.full(mbuf.shape, -jnp.inf, F32)
    acc[...] = jnp.zeros(acc.shape, F32)


    scales = []
    for c in range(NC):
        rows = rows_of(c)
        parts = []
        for d in range(1, X):
            send_tok(d, c).wait_recv()
            relay_tok(d, c).start()
            parts.append(feature_part(rows, ((chip - d + X) % X) * 2 + core))
        if c == 1:
            for w in loads[2:]:
                w.wait()
            v_t[...] = w_v[...].astype(F32).T.astype(BF)
        if c:
            conv_in(c - 1, scales[c - 1])
        for d in range(1, X):
            relay_tok(d, c).wait_recv()
            parts.append(feature_part(rows, ((chip - d + X) % X) * 2 + 1 - core))
        scales.append(latents(c, parts))
        kv_start(c)
        if c and c - 1 < BC:
            queries(c - 1, scales[c - 1])
        if c >= 1:
            lines(c - 1, near)
        if c >= 2:
            lines(c - 2, far)
        if c and c - 1 < BC:
            gate_in(c - 1, scales[c - 1])
        if c == NC - 1:
            conv_in(c, scales[c])
            send_halo(0).start()
            send_halo(1).start()
        if c >= 1:
            crosses(c - 1, [0])
        if c >= 2:
            crosses(c - 2, near)
    first_q = (chip + 1) % X
    take(0, [0])
    heed(first_q, 0, [0])
    crosses(0, far)
    lines(2, far)
    lines(3, near)
    crosses(3, [0])
    crosses(2, near)
    take(0, cross)
    take(1, [0])
    attend(first_q, [line(0, t) for t in cross] + [line(1, 0)])
    crosses(1, far)
    lines(3, far)
    take(2, [0])
    take(1, cross)
    crosses(3, near)
    crosses(2, far)
    attend(first_q, [line(1, t) for t in cross] + [line(2, 0)])
    take(3, [0])
    crosses(3, far)
    take(2, cross)
    attend(first_q, [line(2, t) for t in cross] + [line(3, 0)])
    conv_out()
    take(3, cross)
    heed(first_q, 3, cross)
    finish(first_q)
    for d in range(1, X):
        project_out(d)
        kq = (chip + d + 1) % X
        if d == 1:
            for c in range(BC, NC):
                queries(c, scales[c])
                gate_in(c, scales[c])
        for c in range(NC):
            chunks(kq, c, c + 1)
        finish(kq)
    project_out(0)

    for i in range(NP):
        total = pair_sum(0, i)
        for d in range(1, X):
            send_x(d, i).wait_recv()
            total = total + rbuf[d, i].astype(F32)
        obuf[i] = total.astype(BF)
        give(i).start()

    def sent(ref, sem):
        pltpu.make_async_copy(ref, ref, sem).wait()

    for d in range(X):
        sent(x_all.at[:, cols(tp)], tsend.at[d])
        sent(send_b.at[d], dsend.at[d])
        if d:
            sent(x_all.at[:, cols(tp)], rsend.at[d])
            sent(xbuf.at[d], xsend.at[d])
    sent(kv.at[:, core, 0, pl.ds(0, Z - 1)], zsend.at[0])
    sent(kv.at[:, core, pl.ds(0, Y - 1)], ysend.at[0])
    sent(kv.at[:, core], msend.at[0])
    send_halo(0).wait_send()
    send_halo(1).wait_send()
    for i in range(NP):
        give(i).wait()
def on_device(n_sp, n_tp, tokens, wci, wcn, wco, wcg, taps, wq, wl, wr, gain, ku, vu, wg, cd, ad):
    R, fl = tokens.shape
    D, C = wci.shape
    KV = wl.shape[1]
    H = ku.shape[1] // NOPE
    A = H * VDIM
    X = n_tp // 2
    Y = X if n_sp % X == 0 else 1
    Z = n_sp // Y
    RG, TB = R // X, R // n_tp
    NC, NP = 4, 4
    RC = R // NC
    DP = D // NP
    S = n_sp * R
    KB = min(512, n_sp * RC)
    dma = pltpu.SemaphoreType.DMA
    anys = pl.BlockSpec(memory_space=pl.ANY)
    vm = pl.BlockSpec(memory_space=pltpu.VMEM)
    V = pltpu.VMEM
    return pl.pallas_call(
        functools.partial(body, (n_sp, n_tp, Y, Z, R, fl, D, H, C, KV, NC, NP, KB)),
        out_shape=jax.ShapeDtypeStruct((TB, cd.shape[1]), BF),
        in_specs=[anys] * 13 + [vm] * 2,
        out_specs=anys,
        scratch_shapes=[
            V((R, D), BF), V((4, D, C), BF), V(wq.shape, BF), V((D, A), BF),
            V((D, KV), BF), V((ROPE, D), BF), V(ku.shape, BF), V(vu.shape, BF),
            V((A, KV), BF), V((C + A, cd.shape[1]), BF),
            V((NC, 2, Y, Z, RC + RC // 8, LANES), BF),
            V((S, H * NOPE), BF), V((S, LANES), BF), V((H, VROWS, S), BF), V((X, H, 2 * LANES, RG), BF),
            V((R, LANES), F32), V((R, LANES), F32), V((R, LANES), F32), V((4, 8, R), F32),
            V((R, C), BF), V((R, C), F32), V((R, A), F32), V((2, EDGE, C), BF), V((R, C + A), BF),
            V((X, H, 1, RG), F32), V((X, H, VROWS, RG), F32), V((3, KB, RG), F32),
            V((X, NP, TB, DP), BF), V((X, NP, TB, DP), BF),
            V((X, NP, TB, DP), BF), V((X, NP, TB, DP), BF), V((NP, TB, DP), BF), V((NP, TB, DP), BF),
            V((R, KV), F32), V((R, ROPE), F32), V((R, 1), F32),
            dma((13,)), dma((X,)), dma((X, NC)), dma((X,)), dma((X, NC)),
            dma((1,)), dma((NC, Z)), dma((1,)), dma((NC, Y, Z)), dma((1,)), dma((NC, Y)),
            dma((2,)), dma((2,)),
            dma((X,)), dma((X, NP)), dma((X,)), dma((X, NP)), dma((NP,)),
        ],
        compiler_params=pltpu.CompilerParams(
            collective_id=0, has_side_effects=True, vmem_limit_bytes=60 * 1024 * 1024),
    )(tokens, wci, wcn, wco, wcg, wq, wg, wl, wr.T, cd, ad, ku, vu, taps, gain.reshape(1, KV))


def solution(mesh):
    tp = P(None, "tp")
    placed = (P("sp", "tp"), tp, tp, tp, tp, tp, tp, P(), P(), P(), tp, tp, tp,
              P("tp", None), P("tp", None))
    return jax.shard_map(
        functools.partial(on_device, mesh.shape["sp"], mesh.shape["tp"]),
        mesh=mesh, in_specs=placed, out_specs=P(("sp", "tp"), None), check_vma=False)
```

time: 55.6 us -> 53.5 us (0.962)
  Pallas kernels: 53.6 us -> 51.4 us
    pallas_call x1, Pallas kernels: 53.6 us -> 51.4 us  [on_device(): pl.pallas_call(functools.partial(body, (n_sp, n_tp, Y, Z, R, fl, D, H, C,...]
where the time goes in v2:
time: 53.5 us; the launch traced here: 53.3 us
  Pallas kernels  51.4 us (96%)
  local copies, waits for them, and re-layouts  1.88 us (4%)
    pallas_call x1, Pallas kernels, on_device(): pl.pallas_call(functools.partial(body, (n_sp, n_tp, Y, Z, R, fl, D, H, C,...  51.4 us
    unnamed x1, local copies, waits for them, and re-layouts  1.88 us

profile of v2, /device:TPU:0, one launch (start us, length us, event | category | flops | bytes accessed | tf_op | source)
XLA Modules:
  0.0 53.3 jit_solution(5876045527913026403)
XLA Ops:
  0.0 51.4 %shard_map.145 = bf16[128,2048]{1,0:T(8,128)(2,1)} custom-call(bf16[512,512]{1,0:T(8,128)(2,1)} %tokens.1, bf16[2048,256]{1,0:T(8,128)(2,1)} %wci.1, bf16[2048,256]{1,0:T(8,128)(2,1)} %wcn.1, bf16[2048,256]{1,0:T(8,128)(2,1)} %wco.1, bf16[2048,256]{1,0:T(8,128)(2,1)} %wcg.1, bf16[2048,384]{1,0:T(8,128)(2,1)} %wq.1, bf16[2048,256]{1,0:T(8,128)(2,1)} %wg.1, ...), custom_call_target="tpu_custom_call" | custom-call | tf_op jit(solution)/shard_map/pallas_call | solution.py:543
  51.4 1.9 %copy.17 = bf16[128,2048]{1,0:T(8,128)(2,1)} copy(bf16[128,2048]{1,0:T(8,128)(2,1)} %shard_map.145) | data formatting | bytes 1048576

commit v3 on v2

--- a/solution.py
+++ b/solution.py
@@ -465,18 +465,18 @@
     crosses(0, far)
     lines(2, far)
     lines(3, near)
-    crosses(3, [0])
+    take(1, [0])
+    take(0, cross)
     crosses(2, near)
-    take(0, cross)
-    take(1, [0])
     attend(first_q, [line(0, t) for t in cross] + [line(1, 0)])
     crosses(1, far)
     lines(3, far)
     take(2, [0])
+    crosses(3, [0])
     take(1, cross)
-    crosses(3, near)
     crosses(2, far)
     attend(first_q, [line(1, t) for t in cross] + [line(2, 0)])
+    crosses(3, near)
     take(3, [0])
     crosses(3, far)
     take(2, cross)

time: 53.5 us -> 52.9 us (0.989)
  Pallas kernels: 51.4 us -> 50.8 us
    pallas_call x1, Pallas kernels: 51.4 us -> 50.8 us  [on_device(): pl.pallas_call(functools.partial(body, (n_sp, n_tp, Y, Z, R, fl, D, H, C,...]
where the time goes in v3:
time: 52.9 us; the launch traced here: 52.7 us
  Pallas kernels  50.8 us (96%)
  local copies, waits for them, and re-layouts  1.88 us (4%)
    pallas_call x1, Pallas kernels, on_device(): pl.pallas_call(functools.partial(body, (n_sp, n_tp, Y, Z, R, fl, D, H, C,...  50.8 us
    unnamed x1, local copies, waits for them, and re-layouts  1.88 us

profile of v3, /device:TPU:0, one launch (start us, length us, event | category | flops | bytes accessed | tf_op | source)
XLA Modules:
  0.0 52.7 jit_solution(1292486919516786097)
XLA Ops:
  0.0 50.8 %shard_map.145 = bf16[128,2048]{1,0:T(8,128)(2,1)} custom-call(bf16[512,512]{1,0:T(8,128)(2,1)} %tokens.1, bf16[2048,256]{1,0:T(8,128)(2,1)} %wci.1, bf16[2048,256]{1,0:T(8,128)(2,1)} %wcn.1, bf16[2048,256]{1,0:T(8,128)(2,1)} %wco.1, bf16[2048,256]{1,0:T(8,128)(2,1)} %wcg.1, bf16[2048,384]{1,0:T(8,128)(2,1)} %wq.1, bf16[2048,256]{1,0:T(8,128)(2,1)} %wg.1, ...), custom_call_target="tpu_custom_call" | custom-call | tf_op jit(solution)/shard_map/pallas_call | solution.py:543
  50.8 1.9 %copy.17 = bf16[128,2048]{1,0:T(8,128)(2,1)} copy(bf16[128,2048]{1,0:T(8,128)(2,1)} %shard_map.145) | data formatting | bytes 1048576
